TPU v7x, 128 devices: a 2x2x16 block of a 8x8x16 slice. The times are simulated.
128 devices in a mesh: grp: 4 (over y, x), ep: 32 (over z, core).
Axes of the slice: x: 2, y: 2, z: 16, core: 2. Of those that a mesh axis runs over, the one named last changes fastest.
The devices are a block of a 8x8x16 slice.
Arguments:
- tokens: bfloat16 [2048, 2048], P(('grp', 'ep')), parts along dimension 0, may hold values from -6 to 6
- norm_gain: bfloat16 [2048], replicated, may hold values from 0.099609375 to 1.8984375
- query_weight: bfloat16 [2048, 1024], P(None, 'ep'), may hold values from -0.125 to 0.125
- key_weight: bfloat16 [2048, 256], replicated, may hold values from -0.25 to 0.25
- value_weight: bfloat16 [2048, 256], replicated, may hold values from -0.125 to 0.125
- out_weight: bfloat16 [1024, 2048], P(None, 'ep'), may hold values from -0.1875 to 0.1875
- head_gain: bfloat16 [128], replicated, may hold values from 0.099609375 to 1.8984375
- lambdas: float32 [8], replicated, may hold values from 0.3 to 0.8
- cache_keys: bfloat16 [2048, 1024, 2, 128], P(('grp', 'ep')), parts along dimension 0, may hold values from -1000 to 1000
- cache_values: bfloat16 [2048, 1024, 2, 128], P(('grp', 'ep')), parts along dimension 0, may hold values from -6 to 6
- lengths: int32 [2048], P(('grp', 'ep')), parts along dimension 0, may hold values from 64 to 1024
- moe_gain: bfloat16 [2048], replicated, may hold values from 0.099609375 to 1.8984375
- gate_weight: bfloat16 [32, 2048, 1024], P('ep'), may hold values from -0.375 to 0.375
- up_weight: bfloat16 [32, 2048, 1024], P('ep'), may hold values from -0.375 to 0.375
- down_weight: bfloat16 [32, 1024, 2048], P('ep'), may hold values from -0.02734375 to 0.02734375
- routes: int32 [2048, 4], P(('grp', 'ep')), parts along dimension 0, may hold values from 0 to 31, all different within a row; in each aligned block of 16 rows (0 to 15, 16 to 31, ...) at most 4 rows name the same one
- route_weights: float32 [2048, 4], P(('grp', 'ep')), parts along dimension 0, may hold values from 0.2 to 1
Outputs:
- mixed: bfloat16 [2048, 2048], P(('grp', 'ep')), parts along dimension 0
There are 4 independent parts, one for each index of `grp`. A program takes and returns all parts, laid end to end along the dimension named above; an argument that names none is the same for every part. Nothing has to cross between parts.
Inputs may be any that keep to these rules, and one draw needn't show every extreme that they name: `routes`: a token's 4 experts differ; the tokens of one device name each expert at most 4 times, and in every draw some expert is named exactly 4 times by one device's tokens.
All inputs are finite; a program needn't handle non-finite values.
Results may differ from a plain program's by a relative error of at most 0.034.
Values may be sent and summed in bfloat16 or wider, within the bound.
A program may use at most 128 MiB of HBM per device.

v0:
```python
import jax
import jax.numpy as jnp
from jax import lax
from jax.sharding import Mesh
from jax.sharding import PartitionSpec as P

EP = ("ep_0", "ep_1")
GRP_EP = ("grp", "ep_0", "ep_1")


epsilon = 1e-06
masked_score = -1e30
clamp_limit = 7.0
swish_alpha = 1.702


def in_blocks(value, dim, length):
    before, after = (value.shape[:dim], value.shape[dim + 1 :])
    return jnp.moveaxis(value.reshape(*before, length, -1, *after), dim, 0)


def joined_along(blocks, dim):
    blocks = jnp.moveaxis(blocks, 0, dim)
    lengths = blocks.shape
    return blocks.reshape(*lengths[:dim], lengths[dim] * lengths[dim + 1], *lengths[dim + 2 :])


def moved_by_axis(blocks, axes, sequence):
    inside = blocks.shape[1:]
    filled = blocks.reshape(*(lax.axis_size(a) for a in axes), *inside)
    for k in sequence:
        filled = lax.all_to_all(filled, axes[k], k, k, tiled=True)
    return filled.reshape(-1, *inside)


def two_step_exchange(value, groups, sequence, split_dim, concat_dim):
    length = lax.axis_size(groups[0]) * lax.axis_size(groups[1])
    blocks = in_blocks(value, split_dim, length)
    return joined_along(moved_by_axis(blocks, groups, sequence), concat_dim)


def rms_scaled(values, gain):
    floats = values.astype(jnp.float32)
    return (
        floats
        * lax.rsqrt(jnp.mean(floats * floats, axis=-1, keepdims=True) + epsilon)
        * gain.astype(jnp.float32)
    )


def attention(queries, new_keys, new_values, cache_keys, cache_values, lengths, lambdas, head_gain):
    count = queries.shape[0]
    ctx_len = cache_keys.shape[1]
    kv_count = cache_keys.shape[2]
    head_dim = cache_keys.shape[3] // 2
    heads = lambdas.shape[0]
    group = heads // kv_count
    val_dim = cache_values.shape[3]
    query_grid = queries.reshape(count, kv_count, group, 2, head_dim)
    key_grid = cache_keys.reshape(count, ctx_len, kv_count, 2, head_dim)
    own_keys = new_keys.reshape(count, kv_count, 2, head_dim)
    inv_scale = head_dim ** (-0.5)
    scores = (
        jnp.einsum("bkgcd,bjkcd->bkgcj", query_grid, key_grid, preferred_element_type=jnp.float32)
        * inv_scale
    )
    own_score = (
        jnp.einsum("bkgcd,bkcd->bkgc", query_grid, own_keys, preferred_element_type=jnp.float32)
        * inv_scale
    )
    visible = jnp.arange(ctx_len, dtype=jnp.int32)[None, :] < lengths[:, None]
    scores = jnp.where(visible[:, None, None, None, :], scores, masked_score)
    highest = jnp.maximum(jnp.max(scores, axis=-1), own_score)
    expd = jnp.exp(scores - highest[..., None])
    own_exp = jnp.exp(own_score - highest)
    denominator = jnp.sum(expd, axis=-1) + own_exp
    probs = expd / denominator[..., None]
    own_prob = own_exp / denominator
    lambda_grid = lambdas.reshape(kv_count, group)[None, :, :]
    weights = (probs[:, :, :, 0] - lambda_grid[..., None] * probs[:, :, :, 1]).astype(jnp.bfloat16)
    own_weight = (own_prob[..., 0] - lambda_grid * own_prob[..., 1]).astype(jnp.bfloat16)
    attended = jnp.einsum(
        "bkgj,bjkv->bkgv", weights, cache_values, preferred_element_type=jnp.float32
    )
    own_vals = new_values.reshape(count, kv_count, val_dim).astype(jnp.float32)
    attended = attended + own_weight.astype(jnp.float32)[..., None] * own_vals[:, :, None, :]
    return rms_scaled(attended, head_gain).reshape(count, heads * val_dim).astype(jnp.bfloat16)


def expert_mlp(inputs, gate_w, up_w, down_w):
    gate = jnp.dot(inputs, gate_w, preferred_element_type=jnp.float32)
    upper = jnp.dot(inputs, up_w, preferred_element_type=jnp.float32)
    gate = jnp.minimum(gate, clamp_limit)
    upper = jnp.clip(upper, -clamp_limit, clamp_limit)
    act = ((upper + 1.0) * gate * jax.nn.sigmoid(swish_alpha * gate)).astype(jnp.bfloat16)
    return jnp.dot(act, down_w, preferred_element_type=jnp.float32).astype(jnp.bfloat16)


def local(
    tokens,
    norm_gain,
    query_weight,
    key_weight,
    value_weight,
    out_weight,
    head_gain,
    lambdas,
    cache_keys,
    cache_values,
    lengths,
    moe_gain,
    gate_weight,
    up_weight,
    down_weight,
    routes,
    route_weights,
):
    count = tokens.shape[0]
    width = tokens.shape[1]
    topk = routes.shape[1]
    normed = rms_scaled(tokens, norm_gain).astype(jnp.bfloat16)
    new_keys = jnp.dot(normed, key_weight, preferred_element_type=jnp.float32).astype(jnp.bfloat16)
    new_values = jnp.dot(normed, value_weight, preferred_element_type=jnp.float32).astype(
        jnp.bfloat16
    )
    queries = jnp.dot(
        normed,
        lax.all_gather(query_weight, EP, axis=1, tiled=True),
        preferred_element_type=jnp.float32,
    ).astype(jnp.bfloat16)
    head_out = attention(
        queries, new_keys, new_values, cache_keys, cache_values, lengths, lambdas, head_gain
    )
    attn_out = jnp.dot(
        head_out,
        lax.all_gather(out_weight, EP, axis=1, tiled=True),
        preferred_element_type=jnp.float32,
    ).astype(jnp.bfloat16)
    residual = (tokens.astype(jnp.float32) + attn_out.astype(jnp.float32)).astype(jnp.bfloat16)
    moe_in = rms_scaled(residual, moe_gain).astype(jnp.bfloat16)
    experts = lax.axis_size(EP)
    capacity = min(count, max(2, 2 * count * topk // experts))
    onehot = (routes.reshape(-1)[:, None] == jnp.arange(experts, dtype=jnp.int32)[None, :]).astype(
        jnp.int32
    )
    earlier_all = jnp.cumsum(onehot, axis=0) - onehot
    ranks = jnp.sum(earlier_all * onehot, axis=1).reshape(count, topk)
    slot_id = routes * capacity + ranks
    slot_range = jnp.arange(experts * capacity, dtype=jnp.int32)
    dispatch = jnp.any(slot_id[None, :, :] == slot_range[:, None, None], axis=2).astype(
        jnp.bfloat16
    )
    outgoing = jnp.dot(dispatch, moe_in, preferred_element_type=jnp.float32).astype(jnp.bfloat16)
    outgoing = outgoing.reshape(experts, capacity, width)
    received = lax.all_to_all(outgoing, EP, split_axis=0, concat_axis=0, tiled=True)
    flat_rows = received.reshape(-1, width)
    results = expert_mlp(flat_rows, gate_weight[0], up_weight[0], down_weight[0]).reshape(
        received.shape
    )
    returned = two_step_exchange(results, ("ep_0", "ep_1"), (1, 0), 0, 0)
    picked = returned.reshape(-1, width)[slot_id].astype(jnp.float32)
    moe_sum = jnp.sum(route_weights[:, :, None] * picked, axis=1)
    return (residual.astype(jnp.float32) + moe_sum).astype(jnp.bfloat16)


def solution(mesh):
    torus = Mesh(mesh.devices.reshape(mesh.shape["grp"], 16, 2), ("grp", "ep_0", "ep_1"))
    return jax.shard_map(
        local,
        mesh=torus,
        in_specs=(
            P(GRP_EP, None),
            P(),
            P(None, EP),
            P(),
            P(),
            P(None, EP),
            P(),
            P(),
            P(GRP_EP, None, None, None),
            P(GRP_EP, None, None, None),
            P(GRP_EP),
            P(),
            P(EP, None, None),
            P(EP, None, None),
            P(EP, None, None),
            P(GRP_EP, None),
            P(GRP_EP, None),
        ),
        out_specs=P(GRP_EP, None),
        check_vma=False,
    )
```

profile of v0, /device:TPU:70, one launch (start us, length us, event | category | flops | bytes accessed | tf_op | source)
XLA Modules:
  0.0 256.2 jit_solution(1029286353424995351)
XLA Ops:
  6.6 0.7 all-gather.3.cloned.1.call-update
  7.4 0.7 all-gather.5.cloned.1.call-update
  8.1 0.7 convert_element_type.86
  8.8 1.0 fusion.57
  9.8 1.1 convolution_convert_fusion.4
  11.1 21.3 %copy.77 = bf16[16,1024,2,128]{1,3,2,0:T(8,128)(2,1)} copy(bf16[16,1024,2,128]{3,2,1,0:T(2,128)(2,1)} %param.25) | data formatting | bytes 16777216 | tf_op args[8]
  33.7 51.6 %all-gather.3.cloned.1.call-done = bf16[2048,1024]{0,1:T(8,128)(2,1)} async-done(((bf16[2048,32]{0,1:T(8,128)(2,1)}), bf16[2048,1024]{0,1:T(8,128)(2,1)}) %all-gather.3.cloned.1.call-update) | async-done | bytes 4194320 | tf_op jit(solution)/shard_map/all_gather | solution.py:128
  85.4 3.4 %convolution_convert_fusion.2 = bf16[16,1024]{1,0:T(8,128)(2,1)S(1)} fusion(bf16[2048,1024]{0,1:T(8,128)(2,1)} %all-gather.3.cloned.1.call-done, bf16[16,2048]{1,0:T(8,128)(2,1)S(1)} %copy-done.1, f32[2048]{0:T(1024)S(1)} %convert_element_type.86, f32[16]{0:T(128)S(1)} %add_rsqrt_fusion.2), kind=kOutput, calls=%fused_computation.26 | convolution fusion | flops 67256320 | bytes 4300864 | tf_op jit(solution)/shard_map/dot_general | solution.py:126
  89.2 4.7 %fusion.81 = (f32[16,2,4,2]{2,3,1,0:T(2,128)S(1)}, f32[16,2,4,2,1024]{4,2,3,1,0:T(4,128)S(1)}) fusion(bf16[16,1024,2,2,64]{1,4,3,2,0:T(8,128)(2,1)} %bitcast.96, bf16[16,2,4,2,64]{4,3,2,1,0:T(2,128)(2,1)S(1)} %reshape.79, pred[16,1024]{1,0:T(8,128)(4,1)S(1)} %iota_compare_fusion), kind=kOutput, calls=%fused_computation.91 | convolution fusion | flops 34340608 | bytes 9487360 | tf_op jit(solution)/shard_map/bkgcd,bjkcd->bkgcj/dot_general | solution.py:64
  94.1 0.5 fusion.40
  95.1 0.5 fusion.39
  95.6 5.0 %multiply_reduce_fusion.2 = (f32[16,2,4]{2,1,0:T(2,128)S(1)}, f32[16,2,4,128]{3,2,1,0:T(4,128)S(1)}) fusion(f32[16,2,128]{2,1,0:T(2,128)S(1)} %reshape.86, f32[16,2,4]{2,1,0:T(2,128)S(1)} %copy.85, bf16[16,1024,2,128]{3,2,1,0:T(2,128)(2,1)} %param.26, f32[16,2,4,2,1024]{4,2,3,1,0:T(4,128)S(1)} %fusion.39, f32[2,4]{1,0:T(2,128)S(1)} %mul.149), kind=kOutput, calls=%fused_computation.60 | convolution fusion | flops 34013056 | bytes 9520160 | tf_op jit(solution)/shard_map/bkgj,bjkv->bkgv/dot_general | solution.py:82
  100.9 53.7 %all-gather.5.cloned.1.call-done = bf16[1024,2048]{0,1:T(8,128)(2,1)} async-done(((bf16[1024,64]{0,1:T(8,128)(2,1)}), bf16[1024,2048]{0,1:T(8,128)(2,1)}) %all-gather.5.cloned.1.call-update) | async-done | bytes 4194320 | tf_op jit(solution)/shard_map/all_gather | solution.py:136
  154.6 3.5 %multiply_reduce_fusion.1 = (f32[16]{0:T(128)S(1)}, f32[16,2048]{1,0:T(8,128)S(1)}) fusion(bf16[16,1024]{1,0:T(8,128)(2,1)S(1)} %convert_element_type.97, bf16[1024,2048]{0,1:T(8,128)(2,1)} %all-gather.5.cloned.1.call-done, bf16[16,2048]{1,0:T(8,128)(2,1)S(1)} %copy-done.1), kind=kOutput, calls=%fused_computation.56 | convolution fusion | flops 67370992 | bytes 4423744 | tf_op jit(solution)/shard_map/dot_general | solution.py:134
  158.7 42.0 %all_to_all.15 = bf16[32,4,2048]{2,1,0:T(4,128)(2,1)S(1)} all-to-all(bf16[32,4,2048]{2,1,0:T(4,128)(2,1)S(1)} %reshape.83), channel_id=1, replica_groups=mesh['grp'=4,'ep_0'=16,'ep_1'=2] {'ep_0','ep_1'}, dimensions={0} | all-to-all | bytes 1048576 | tf_op jit(solution)/shard_map/all_to_all | solution.py:155
  200.8 2.9 %fusion.20 = f32[128,1024]{1,0:T(8,128)S(1)} fusion(bf16[128,2048]{1,0:T(8,128)(2,1)S(1)} %reshape.84, bf16[1,2048,1024]{2,1,0:T(8,128)(2,1)} %param.29), kind=kOutput, calls=%fused_computation.20 | convolution fusion | flops 537001984 | bytes 5242880 | tf_op jit(solution)/shard_map/dot_general | solution.py:91
  203.7 4.9 %fusion.8 = bf16[128,2048]{1,0:T(8,128)(2,1)S(1)} fusion(bf16[1,1024,2048]{2,1,0:T(8,128)(2,1)} %param.31, f32[128,1024]{1,0:T(8,128)S(1)} %fusion.20, bf16[128,2048]{1,0:T(8,128)(2,1)S(1)} %reshape.84, bf16[1,2048,1024]{2,1,0:T(8,128)(2,1)} %param.30), kind=kOutput, calls=%fused_computation.9 | convolution fusion | flops 1075183616 | bytes 9961472 | tf_op jit(solution)/shard_map/dot_general | solution.py:96
  209.0 4.2 %all_to_all.16 = bf16[16,2,1,4,2048]{4,3,0,2,1:T(4,128)(2,1)S(1)} all-to-all(bf16[16,2,1,4,2048]{4,3,0,2,1:T(4,128)(2,1)S(1)} %copy.92), channel_id=1, replica_groups=mesh['grp'=4,'ep_0'=16,'ep_1'=2] {'ep_1'}, dimensions={1} | all-to-all | bytes 1048576 | tf_op jit(solution)/shard_map/all_to_all | solution.py:32
  213.2 1.0 copy.93
  214.2 4.0 %all-to-all-start.2 = ((bf16[16,2,1,4,2048]{4,3,1,2,0:T(4,128)(2,1)}), bf16[16,2,1,4,2048]{4,3,1,2,0:T(4,128)(2,1)S(1)}, u32[]{:S(2)}, u32[]{:S(2)}) async-start(bf16[16,2,1,4,2048]{4,3,1,2,0:T(4,128)(2,1)} %copy.93), calls=%async_computation.2 | async-start | bytes 1048576 | tf_op jit(solution)/shard_map/all_to_all | solution.py:32
  218.4 28.8 %all-to-all-done.2 = bf16[16,2,1,4,2048]{4,3,1,2,0:T(4,128)(2,1)S(1)} async-done(((bf16[16,2,1,4,2048]{4,3,1,2,0:T(4,128)(2,1)}), bf16[16,2,1,4,2048]{4,3,1,2,0:T(4,128)(2,1)S(1)}, u32[]{:S(2)}, u32[]{:S(2)}) %all-to-all-start.2) | async-done | bytes 524320 | tf_op jit(solution)/shard_map/all_to_all | solution.py:32
  247.4 0.7 gather_fusion
  248.3 0.4 multiply_reduce_fusion
  248.7 0.6 add_convert_fusion
  (64 shorter events, 4.4 us)
Async XLA Ops:
  6.5 3.2 %copy-start = (bf16[2048,256]{1,0:T(8,128)(2,1)S(1)}, bf16[2048,256]{1,0:T(8,128)(2,1)}, u32[]{:S(2)}) copy-start(bf16[2048,256]{1,0:T(8,128)(2,1)} %param.20) | copy-start | bytes 3145732
  6.6 78.8 %all-gather.3.cloned.1.call-start = ((), (), s32[]{:S(2)}) async-start(), calls=%async_computation.3 | async-start | bytes 4325376 | tf_op jit(solution)/shard_map/all_gather | solution.py:128
  7.3 147.3 %all-gather.5.cloned.1.call-start = ((), (), s32[]{:S(2)}) async-start(), calls=%async_computation.4 | async-start | bytes 4325376 | tf_op jit(solution)/shard_map/all_gather | solution.py:136
  11.0 21.4 %copy-start.7 = (f32[8]{0:T(128)S(1)}, f32[8]{0:T(128)}, u32[]{:S(2)}) copy-start(f32[8]{0:T(128)} %param.24) | copy-start | bytes 100
  11.0 21.4 %copy-start.1 = (bf16[16,2048]{1,0:T(8,128)(2,1)S(1)}, bf16[16,2048]{1,0:T(8,128)(2,1)}, u32[]{:S(2)}) copy-start(bf16[16,2048]{1,0:T(8,128)(2,1)} %param.17) | copy-start | bytes 196612
  11.0 21.4 %copy-start.2 = (bf16[2048,256]{1,0:T(8,128)(2,1)S(1)}, bf16[2048,256]{1,0:T(8,128)(2,1)}, u32[]{:S(2)}) copy-start(bf16[2048,256]{1,0:T(8,128)(2,1)} %param.21) | copy-start | bytes 3145732
  11.0 21.7 %copy-start.8 = (bf16[128]{0:T(256)(128)(2,1)S(1)}, bf16[128]{0:T(256)(128)(2,1)}, u32[]{:S(2)}) copy-start(bf16[128]{0:T(256)(128)(2,1)} %param.23) | copy-start | bytes 772
  11.1 21.7 %copy-start.4 = (s32[16,4]{0,1:T(4,128)S(1)}, s32[16,4]{0,1:T(4,128)}, u32[]{:S(2)}) copy-start(s32[16,4]{0,1:T(4,128)} %param.32) | copy-start | bytes 772
  11.1 22.5 %copy-start.3 = (bf16[2048]{0:T(1024)(128)(2,1)S(1)}, bf16[2048]{0:T(1024)(128)(2,1)}, u32[]{:S(2)}) copy-start(bf16[2048]{0:T(1024)(128)(2,1)} %param.28) | copy-start | bytes 12292
  11.1 22.5 %copy-start.6 = (s32[16]{0:T(128)S(1)}, s32[16]{0:T(128)}, u32[]{:S(2)}) copy-start(s32[16]{0:T(128)} %param.27) | copy-start | bytes 196
  208.6 9.8 %copy-start.5 = (f32[16,4]{0,1:T(4,128)S(1)}, f32[16,4]{0,1:T(4,128)}, u32[]{:S(2)}) copy-start(f32[16,4]{0,1:T(4,128)} %param.33) | copy-start | bytes 772
  214.2 33.0 %all-to-all-start.2 = ((bf16[16,2,1,4,2048]{4,3,1,2,0:T(4,128)(2,1)}), bf16[16,2,1,4,2048]{4,3,1,2,0:T(4,128)(2,1)S(1)}, u32[]{:S(2)}, u32[]{:S(2)}) async-start(bf16[16,2,1,4,2048]{4,3,1,2,0:T(4,128)(2,1)} %copy.93), calls=%async_computation.2 | async-start | bytes 1048576 | tf_op jit(solution)/shard_map/all_to_all | solution.py:32
Sparse Core Ops, SparseCore 0:
  9.1 76.2 all-gather.2
  87.1 67.4 all-gather.4
where the time goes:
time: 258 us; the launch traced here: 256 us
  waiting for transfers between devices  136 us (53%)
  blocking collectives  46.1 us (18%)
  matrix products  26.3 us (10%)
  local copies, waits for them, and re-layouts  25.8 us (10%)
  between operations  13.7 us (5%)
  other arithmetic  4.51 us (2%)
  starting transfers between devices  4.08 us (2%)
    all_gather x1, waiting for transfers between devices, local(): lax.all_gather(out_weight, EP, axis=1, tiled=True)  53.7 us
    all_gather x1, waiting for transfers between devices, local(): lax.all_gather(query_weight, EP, axis=1, tiled=True)  51.6 us
    all_to_all x1, blocking collectives, local(): lax.all_to_all(outgoing, EP, split_axis=0, concat_axis=0, tiled=True)  42 us
    all_to_all x1, waiting for transfers between devices, moved_by_axis(): filled = lax.all_to_all(filled, axes[k], k, k, tiled=True)  28.8 us
    unnamed x21, local copies, waits for them, and re-layouts  21.5 us
  transfers between devices with their start and end apart: 3, of which 3 were waited for; matrix products, arithmetic and copies ran while one was open for 16% of the time, Pallas kernels for 0%

commit v1 on v0

v1 whole, which is shorter than its diff:
```python
import functools

import jax
import jax.numpy as jnp
from jax import lax
from jax.experimental import pallas as pl
from jax.experimental.pallas import tpu as pltpu
from jax.sharding import PartitionSpec as P

EPS = 1e-06
NEG = -1e30
LIMIT = 7.0
ALPHA = 1.702
F32 = jnp.float32
BF16 = jnp.bfloat16
MESH = pl.DeviceIdType.MESH
META = 128
PIECES = 2
WO_PIECES = 4
CACHE_STEPS = 4


def iota(shape, dim):
    return lax.broadcasted_iota(jnp.int32, shape, dim)


def mask(cond):
    return jnp.where(cond, 1.0, 0.0).astype(F32)


def dot(a, b, dims=(((1,), (0,)), ((), ()))):
    return lax.dot_general(a, b, dims, preferred_element_type=F32)


def scaled(x, gain):
    return x * lax.rsqrt(jnp.mean(x * x, axis=-1, keepdims=True) + EPS) * gain


def kernel(
    nz, kv, lam_ref, len_ref, tok_ref, ng_ref, hg_ref, mg_ref, routes_ref, rw_ref,
    wq_hbm, wk_hbm, wv_hbm, wo_hbm, keys_hbm, vals_hbm, gate_hbm, up_hbm, down_hbm,
    out_ref,
    kbuf, vbuf, gbuf, ubuf, dbuf, wqb, wqp, wq128, wkb, wvb, wob,
    xg, wog, qs, qr, qall, owns, vown, hof, attn, res, mx, xc, xe, ye, yo, yr, act,
    rf, rin_r, rin_l, st_f, st_w,
    lsem, cache_sem, pair_send, pair_recv,
    x_sr, x_sl, x_rc, wo_sr, wo_sl, wo_rc, wop_s, wop_r, q_s, q_r,
    m_sr, m_sl, m_rc, r_sr, r_sl, r_rr, r_rl,
):
    rows, width = tok_ref.shape
    heads = 2 * nz * 64 // 2 // 64 // 2
    group = heads // kv
    ctx2 = kbuf.shape[1]
    half = nz // 2
    kp = xg.shape[0]
    pw = width // kp
    kw = wo_sr.shape[1]
    me = lax.axis_index("ep")
    z = lax.div(me, 2)
    c = lax.rem(me, 2)

    def wrap(v):
        return lax.rem(v + 2 * nz, nz)

    def dev(zz, cc):
        return {"ep": zz * 2 + cc}

    right = dev(wrap(z + 1), c)
    left = dev(wrap(z - 1), c)
    partner = dev(z, 1 - c)
    sent = []

    def send(src, dst, ssem, rsem, to):
        cp = pltpu.make_async_remote_copy(
            src_ref=src, dst_ref=dst, send_sem=ssem, recv_sem=rsem, device_id=to, device_id_type=MESH
        )
        cp.start()
        sent.append(cp)

    def arrived(dst, rsem, ssem):
        pltpu.make_async_remote_copy(
            src_ref=dst, dst_ref=dst, send_sem=ssem, recv_sem=rsem, device_id=right, device_id_type=MESH
        ).wait_recv()

    loads = {}

    def load(name, src, dst, sem):
        cp = pltpu.make_async_copy(src, dst, sem)
        cp.start()
        loads[name] = cp

    load("wq", wq_hbm, wqb, lsem.at[0])
    load("wo", wo_hbm, wob, lsem.at[1])
    load("wk", wk_hbm, wkb, lsem.at[2])
    load("wv", wv_hbm, wvb, lsem.at[3])
    steps = cache_sem.shape[1]
    per = rows // steps
    for i in range(steps):
        part = pl.ds(i * per, per)
        load(("k", i), keys_hbm.at[part], kbuf.at[part], cache_sem.at[0, i])
        load(("v", i), vals_hbm.at[part], vbuf.at[part], cache_sem.at[1, i])
    load("gate", gate_hbm.at[0], gbuf, lsem.at[4])
    load("up", up_hbm.at[0], ubuf, lsem.at[5])
    load("down", down_hbm.at[0], dbuf, lsem.at[6])

    barrier = pltpu.get_barrier_semaphore()
    for i in range(1, nz):
        pl.semaphore_signal(barrier, inc=1, device_id=dev(wrap(z + i), c), device_id_type=MESH)
    pl.semaphore_signal(barrier, inc=1, device_id=partner, device_id_type=MESH)

    tokens = tok_ref[...].astype(F32)
    normed = scaled(tokens, ng_ref[...].astype(F32)).astype(BF16)
    weight = rw_ref[...]
    topk = weight.shape[1]
    hi = weight.astype(BF16).astype(F32)
    lo = weight - hi
    lane = iota((rows, META), 1)
    meta = jnp.zeros((rows, META), F32)
    routes = routes_ref[...].astype(F32)
    for k in range(topk):
        meta = jnp.where(lane == k, routes[:, k : k + 1], meta)
        meta = jnp.where(lane == topk + k, hi[:, k : k + 1], meta)
        meta = jnp.where(lane == 2 * topk + k, lo[:, k : k + 1], meta)
    for p in range(kp):
        xg[p, 0, :, 0:pw] = normed[:, p * pw : (p + 1) * pw]
        xg[p, 0, :, pw : pw + META] = meta.astype(BF16)

    pl.semaphore_wait(barrier, nz)

    def hop(buf, h, s_r, s_l, r_c):
        for p in range(kp):
            if h >= 1:
                arrived(buf.at[p, h], r_c.at[p, h], s_r.at[p, h - 1])
            if h < half:
                send(buf.at[p, h], buf.at[p, h + 1], s_r.at[p, h], r_c.at[p, h + 1], right)
            if 1 <= h < half:
                arrived(buf.at[p, nz - h], r_c.at[p, nz - h], s_l.at[p, h - 1])
            if h < half - 1:
                back = (nz - h) % nz
                send(buf.at[p, back], buf.at[p, nz - h - 1], s_l.at[p, h], r_c.at[p, nz - h - 1], left)

    wrows = wog.shape[2] // kw

    def wo_task(h, p):
        part = pl.ds(p * wrows, wrows)
        a, b = wrap(z - h), wrap(z + h)
        if h >= 1:
            arrived(wog.at[c, a, part], wo_rc.at[h, p], wo_sr.at[h - 1, p])
        if h < half:
            ref = wog.at[c, a, part]
            send(ref, ref, wo_sr.at[h, p], wo_rc.at[h + 1, p], right)
        if 1 <= h < half:
            arrived(wog.at[c, b, part], wo_rc.at[nz - h, p], wo_sl.at[h - 1, p])
        if h < half - 1:
            ref = wog.at[c, b, part]
            send(ref, ref, wo_sl.at[h, p], wo_rc.at[nz - h - 1, p], left)
        if p == kw - 1:
            send(wog.at[c, a], wog.at[c, a], wop_s.at[h], wop_r.at[h], partner)
            if 1 <= h < half:
                send(wog.at[c, b], wog.at[c, b], wop_s.at[nz - h], wop_r.at[nz - h], partner)

    wo_tasks = [(h, p) for h in range(half + 1) for p in range(kw)]
    done = [0]

    def wo_run(n):
        for h, p in wo_tasks[done[0] : done[0] + n]:
            wo_task(h, p)
        done[0] += n

    def place(off):
        n = wqb.shape[1]
        return mask((iota((n, 128), 1) & 63) == iota((n, 128), 0) + off).astype(BF16)

    hop(xg, 0, x_sr, x_sl, x_rc)
    loads["wq"].wait()
    send(wqb, wqp, pair_send.at[0], pair_recv.at[0], partner)
    loads["wo"].wait()
    kd = wob.shape[0] // 2
    e0 = mask(iota((64, 128), 1) == iota((64, 128), 0)).astype(BF16)
    e1 = mask(iota((64, 128), 1) == iota((64, 128), 0) + 64).astype(BF16)
    wog[c, z] = (dot(wob[0:kd, :], e0) + dot(wob[kd : 2 * kd, :], e1)).astype(BF16)
    wo_run(1)

    nq = wqb.shape[1]
    own_q = dot(wqb[...], place(nq * c))
    arrived(wqp, pair_recv.at[0], pair_send.at[0])
    wq128[...] = (own_q + dot(wqp[...], place(nq * (1 - c)))).astype(BF16)

    lane8 = iota((rows // 2, 128), 1)
    first = lane8 < 64
    odd = lax.rem(z, 2)
    upper = jnp.where(first, 0, 1) == odd

    def query_block(r):
        q = dot(xg[0, r, :, 0:pw], wq128[0:pw, :])
        for p in range(1, kp):
            q = q + dot(xg[p, r, :, 0:pw], wq128[p * pw : (p + 1) * pw, :])
        return jnp.where(upper, q[0 : rows // 2], q[rows // 2 : rows]).astype(BF16)

    def query_send(r):
        qs[r] = query_block(r)
        origin = wrap(z - r)
        send(qs.at[r], qr.at[z], q_s.at[r], q_r.at[z], dev(origin, c))

    hop(xg, 1, x_sr, x_sl, x_rc)
    wo_run(1)
    qr[z] = query_block(0)
    loads["wk"].wait()
    loads["wv"].wait()
    new_keys = dot(normed, wkb[...]).astype(BF16)
    new_vals = dot(normed, wvb[...]).astype(BF16)
    query_send(1)
    query_send(nz - 1)
    for h in range(2, half + 1):
        hop(xg, h, x_sr, x_sl, x_rc)
        if h < half:
            wo_run(1)
        query_send(h)
        if h < half:
            query_send(nz - h)

    nrow = rows * nz
    def rep(n, per_tok, nh, x):
        i0, i1 = iota((n, kv * rows), 0), iota((n, kv * rows), 1)
        tok_i, head_i = lax.div(i0, per_tok), lax.rem(i0, nh)
        sel = (lax.rem(i1, rows) == tok_i) & (lax.div(i1, rows) == lax.div(head_i, group))
        stacked = jnp.concatenate([x[:, i * 128 : (i + 1) * 128] for i in range(kv)], axis=0)
        return dot(mask(sel).astype(BF16), stacked)

    key_rows = rep(nrow, nz, heads, new_keys)
    vown[...] = rep(rows * heads, heads, heads, new_vals).reshape(rows, heads, 128)

    ntok = nz * rows
    mt = xg[0, :, :, pw : pw + META].reshape(ntok, META).astype(F32)
    rt, wt = mt[:, 0:topk], mt[:, topk : 2 * topk] + mt[:, 2 * topk : 3 * topk]
    cap = st_f.shape[1] // (2 * nz)

    def hit(e):
        is_e = mask(rt == e.astype(F32))
        return jnp.sum(is_e, axis=1, keepdims=True), jnp.sum(is_e * wt, axis=1, keepdims=True)

    h0, w0 = hit(me)
    h1, w1 = hit(2 * z + 1 - c)
    ns = st_f.shape[1]
    sl = iota((ntok, ns), 1)
    hb = jnp.where(sl < ns // 2, h0, h1)
    wb = jnp.where(sl < ns // 2, w0, w1)
    t0, t1 = iota((ntok, ntok), 0), iota((ntok, ntok), 1)
    before = mask((lax.div(t0, rows) == lax.div(t1, rows)) & (t1 < t0)).astype(BF16)
    rank = dot(before, hb.astype(BF16))
    slot = (cap * lax.div(iota((ntok, ns), 0), rows)).astype(F32) + rank
    sel = jnp.where((hb > 0.5) & (slot == lax.rem(sl, ns // 2).astype(F32)), 1.0, 0.0)
    st_f[...] = sel
    sw = sel * wb
    sw_hi = sw.astype(BF16)
    st_w[0] = sw_hi
    st_w[1] = (sw - sw_hi.astype(F32)).astype(BF16)

    wo_run(kw)
    for r in range(1, nz):
        src = wrap(z - r)
        arrived(qr.at[src], q_r.at[src], q_s.at[r])
    qf = qr[...].reshape(nz * rows // 2, 128)
    i0 = iota((nz * rows // 2, 128), 0)
    mine = lax.rem(lax.div(i0, rows // 2), 2) == lax.div(iota((nz * rows // 2, 128), 1), 64)
    qf32 = qf.astype(F32)
    q_lo = jnp.where(mine, qf32, 0.0).astype(BF16)
    q_hi = jnp.where(mine, pltpu.roll(qf32, 64, 1), 0.0).astype(BF16)
    qcat = jnp.concatenate([q_lo, q_hi], axis=0)
    o = iota((nrow, nrow), 0)
    ot, oj = lax.div(o, nz), lax.rem(o, nz)
    src_z = 2 * lax.rem(oj, heads) + lax.div(oj, heads)
    hr = rows // 2
    src_row = lax.div(ot, hr) * (nz * hr) + src_z * hr + lax.rem(ot, hr)
    qperm = dot(mask(src_row == iota((nrow, nrow), 1)).astype(BF16), qcat)
    qall[...] = qperm.astype(BF16).reshape(rows, nz, 128)
    scale = 64 ** (-0.5)
    own_score = jnp.sum(qperm * key_rows, axis=1, keepdims=True) * scale
    owns[...] = jnp.broadcast_to(own_score, (nrow, 128)).reshape(rows, nz, 128)

    lam = jnp.zeros((heads, 1), F32)
    for i in range(heads):
        lam = jnp.where(iota((heads, 1), 0) == i, lam_ref[i], lam)
    hgain = hg_ref[...].astype(F32)
    col = iota((nz, ctx2), 1)
    head_of = lax.rem(iota((nz, ctx2), 0), heads)
    kv_ok = lax.rem(col, kv) == lax.div(head_of, group)
    pos = jnp.where(kv_ok, lax.div(col, kv), 1 << 30)

    def attend(t):
        s = dot(qall[t], kbuf[t], (((1,), (1,)), ((), ()))) * scale
        s = jnp.where(pos < len_ref[t], s, NEG)
        own = owns[t][:, 0:1]
        top = jnp.maximum(jnp.max(s, axis=1, keepdims=True), own)
        e = jnp.exp(s - top)
        eo = jnp.exp(own - top)
        den = jnp.sum(e, axis=1, keepdims=True) + eo
        inv = 1.0 / den
        w = (e[0:heads] * inv[0:heads] - (lam * inv[heads:nz]) * e[heads:nz]).astype(BF16)
        wo = (eo[0:heads] * inv[0:heads] - lam * (eo[heads:nz] * inv[heads:nz])).astype(BF16)
        a = dot(w, vbuf[t]) + wo.astype(F32) * vown[t]
        hof[t] = scaled(a, hgain).astype(BF16).astype(F32)

    for i in range(steps):
        wo_run(kw)
        loads[("k", i)].wait()
        loads[("v", i)].wait()

        def body(j, carry):
            attend(i * per + 2 * j)
            attend(i * per + 2 * j + 1)
            return carry

        lax.fori_loop(0, per // 2, body, 0)
    wo_run(len(wo_tasks) - done[0])
    for h in range(half + 1):
        arrived(wog.at[1 - c, wrap(z - h)], wop_r.at[h], wop_s.at[h])
        if 1 <= h < half:
            arrived(wog.at[1 - c, wrap(z + h)], wop_r.at[nz - h], wop_s.at[nz - h])

    hh = heads // 2
    ho = jnp.concatenate(
        [
            jnp.concatenate([hof[:, h, :] for h in range(s * hh, (s + 1) * hh)], axis=1)
            for s in range(2)
        ],
        axis=0,
    ).astype(BF16)
    lo64 = iota((rows, 128), 1) < 64

    def project(j, carry):
        p0 = dot(ho, wog[0, j])
        p1 = dot(ho, wog[1, j])
        direct = jnp.where(lo64, p0[0:rows], p1[rows : 2 * rows])
        turned = jnp.where(lo64, p1[0:rows], p0[rows : 2 * rows])
        attn[j] = direct + pltpu.roll(turned, 64, 1)
        return carry

    lax.fori_loop(0, nz, project, 0)
    total = jnp.zeros((rows, 1), F32)
    for j in range(nz):
        cols = slice(j * 128, (j + 1) * 128)
        v = tok_ref[:, cols].astype(F32) + attn[j].astype(BF16).astype(F32)
        v = v.astype(BF16).astype(F32)
        res[:, cols] = v
        total = total + jnp.sum(v * v, axis=1, keepdims=True)
    inv_rms = lax.rsqrt(total / width + EPS)
    for p in range(kp):
        cols = slice(p * pw, (p + 1) * pw)
        mx[p, 0] = (res[:, cols] * inv_rms * mg_ref[:, cols].astype(F32)).astype(BF16)

    for h in range(half + 1):
        hop(mx, h, m_sr, m_sl, m_rc)

    comp = st_f[...].T.astype(BF16)
    nhalf = ns // 2
    for p in range(kp):
        rows_p = dot(comp, mx[p].reshape(ntok, pw)).astype(BF16)
        xc[p] = rows_p[nhalf:ns]
        send(xc.at[p], xe.at[p, 1], pair_send.at[1 + p], pair_recv.at[1 + p], partner)
        xe[p, 0] = rows_p[0:nhalf]

    loads["gate"].wait()
    loads["up"].wait()
    for p in range(kp):
        arrived(xe.at[p, 1], pair_recv.at[1 + p], pair_send.at[1 + p])
    x = jnp.concatenate([xe[p].reshape(ns, pw) for p in range(kp)], axis=1)
    tile = 256

    def hidden(j, carry):
        cols = pl.ds(pl.multiple_of(j * tile, tile), tile)
        g = jnp.minimum(dot(x, gbuf[:, cols]), LIMIT)
        u = jnp.clip(dot(x, ubuf[:, cols]), -LIMIT, LIMIT)
        act[:, cols] = ((u + 1.0) * g / (1.0 + jnp.exp(-ALPHA * g))).astype(BF16)
        return carry

    lax.fori_loop(0, gbuf.shape[1] // tile, hidden, 0)
    loads["down"].wait()
    av = act[...]
    for p in range(kp):
        y = dot(av, dbuf[:, p * pw : (p + 1) * pw]).astype(BF16)
        ye[p] = y[nhalf:ns]
        send(ye.at[p], yr.at[p], pair_send.at[1 + kp + p], pair_recv.at[1 + kp + p], partner)
        yo[p] = y[0:nhalf]

    for p in range(kp):
        arrived(yr.at[p], pair_recv.at[1 + kp + p], pair_send.at[1 + kp + p])
        yy = jnp.concatenate([yo[p], yr[p]], axis=0)
        r = dot(st_w[0], yy) + dot(st_w[1], yy)
        rf[p] = r.astype(BF16).reshape(nz, rows, pw)
        send(rf.at[p, half], rin_r.at[p, 0], r_sr.at[p, 0], r_rr.at[p, 0], right)
        send(rf.at[p, half - 1], rin_l.at[p, 0], r_sl.at[p, 0], r_rl.at[p, 0], left)

    for t in range(half):
        for p in range(kp):
            arrived(rin_r.at[p, t], r_rr.at[p, t], r_sr.at[p, t])
            if t < half - 1:
                slot_r = half + 1 + t
                rf[p, slot_r] = (rf[p, slot_r].astype(F32) + rin_r[p, t].astype(F32)).astype(BF16)
                send(rf.at[p, slot_r], rin_r.at[p, t + 1], r_sr.at[p, t + 1], r_rr.at[p, t + 1], right)
            if t < half - 1:
                arrived(rin_l.at[p, t], r_rl.at[p, t], r_sl.at[p, t])
            if t < half - 2:
                slot_l = half - 2 - t
                rf[p, slot_l] = (rf[p, slot_l].astype(F32) + rin_l[p, t].astype(F32)).astype(BF16)
                send(rf.at[p, slot_l], rin_l.at[p, t + 1], r_sl.at[p, t + 1], r_rl.at[p, t + 1], left)
    for p in range(kp):
        cols = slice(p * pw, (p + 1) * pw)
        moe = rf[p, 0].astype(F32) + rin_r[p, half - 1].astype(F32) + rin_l[p, half - 2].astype(F32)
        out_ref[:, cols] = (res[:, cols] + moe).astype(BF16)

    for cp in sent:
        cp.wait_send()


def local(
    nz, tokens, norm_gain, query_weight, key_weight, value_weight, out_weight, head_gain, lambdas,
    cache_keys, cache_values, lengths, moe_gain, gate_weight, up_weight, down_weight, routes, route_weights,
):
    rows, width = tokens.shape
    ctx, kv, kd = cache_keys.shape[1:]
    ff = gate_weight.shape[2]
    keys = cache_keys.reshape(rows, ctx * kv, kd)
    vals = cache_values.reshape(rows, ctx * kv, kd)
    heads = lambdas.shape[0]
    half = nz // 2
    kp, kw = PIECES, WO_PIECES
    pw = width // kp
    ns = 2 * nz * 4
    kdim = out_weight.shape[0] // 2
    vmem, smem, anym = (pl.BlockSpec(memory_space=m) for m in (pltpu.VMEM, pltpu.SMEM, pl.ANY))
    dma = pltpu.SemaphoreType.DMA
    V = pltpu.VMEM
    scratch = [
        V(keys.shape, BF16), V(vals.shape, BF16),
        V((width, ff), BF16), V((width, ff), BF16), V((ff, width), BF16),
        V(query_weight.shape, BF16), V(query_weight.shape, BF16), V((width, 128), BF16),
        V(key_weight.shape, BF16), V(value_weight.shape, BF16), V(out_weight.shape, BF16),
        V((kp, nz, rows, pw + META), BF16),
        V((2, nz, kdim, 128), BF16),
        V((nz, rows // 2, 128), BF16), V((nz, rows // 2, 128), BF16),
        V((rows, nz, 128), BF16), V((rows, nz, 128), F32), V((rows, heads, 128), F32),
        V((rows, heads, 128), F32), V((nz, rows, 128), F32), V((rows, width), F32),
        V((kp, nz, rows, pw), BF16),
        V((kp, ns // 2, pw), BF16), V((kp, 2, ns // 2, pw), BF16),
        V((kp, ns // 2, pw), BF16), V((kp, ns // 2, pw), BF16), V((kp, ns // 2, pw), BF16),
        V((ns, ff), BF16),
        V((kp, nz, rows, pw), BF16), V((kp, half, rows, pw), BF16), V((kp, half, rows, pw), BF16),
        V((nz * rows, ns), F32), V((2, nz * rows, ns), BF16),
        dma((7,)), dma((2, CACHE_STEPS)), dma((1 + 2 * kp,)), dma((1 + 2 * kp,)),
        dma((kp, half)), dma((kp, half)), dma((kp, nz)),
        dma((half, kw)), dma((half, kw)), dma((nz, kw)),
        dma((nz,)), dma((nz,)), dma((nz,)), dma((nz,)),
        dma((kp, half)), dma((kp, half)), dma((kp, nz)),
        dma((kp, half)), dma((kp, half)), dma((kp, half)), dma((kp, half)),
    ]
    return pl.pallas_call(
        functools.partial(kernel, nz, kv),
        out_shape=jax.ShapeDtypeStruct((rows, width), BF16),
        in_specs=[smem, smem] + [vmem] * 6 + [anym] * 9,
        out_specs=vmem,
        scratch_shapes=scratch,
        compiler_params=pltpu.CompilerParams(
            collective_id=0, has_side_effects=True, vmem_limit_bytes=60 * 1024 * 1024
        ),
    )(
        lambdas, lengths, tokens, norm_gain.reshape(1, -1), head_gain.reshape(1, -1),
        moe_gain.reshape(1, -1), routes, route_weights,
        query_weight, key_weight, value_weight, out_weight, keys, vals,
        gate_weight, up_weight, down_weight,
    )


def solution(mesh):
    both = ("grp", "ep")
    return jax.shard_map(
        functools.partial(local, mesh.shape["ep"] // 2),
        mesh=mesh,
        in_specs=(
            P(both, None), P(), P(None, "ep"), P(), P(), P(None, "ep"), P(), P(),
            P(both, None, None, None), P(both, None, None, None), P(both), P(),
            P("ep", None, None), P("ep", None, None), P("ep", None, None),
            P(both, None), P(both, None),
        ),
        out_specs=P(both, None),
        check_vma=False,
    )
```

time: 258 us -> 150 us (0.58)
  Pallas kernels: 0 us -> 139 us
  waiting for transfers between devices: 136 us -> 0 us
  blocking collectives: 46.1 us -> 0 us
  matrix products: 26.3 us -> 0 us
  local copies, waits for them, and re-layouts: 25.8 us -> 10.4 us
  between operations: 13.7 us -> 0.01 us
  other arithmetic: 4.51 us -> 0 us
  starting transfers between devices: 4.08 us -> 0 us
    pallas_call x0 -> x1, Pallas kernels: none -> 139 us  [local(): pl.pallas_call(functools.partial(kernel, nz, kv), out_shape=jax.ShapeDtyp...]
    all_gather x2 -> x0, waiting for transfers between devices: 105 us -> none  [the longest x1 53.7 us: local(): lax.all_gather(out_weight, EP, axis=1, tiled=True)]
    all_to_all x2 -> x0, blocking collectives: 46.1 us -> none  [the longest x1 42 us: local(): lax.all_to_all(outgoing, EP, split_axis=0, concat_axis=0, tiled=True)]
    all_to_all x1 -> x0, waiting for transfers between devices: 28.8 us -> none  [moved_by_axis(): filled = lax.all_to_all(filled, axes[k], k, k, tiled=True)]
    dot_general x10 -> x0, matrix products: 26.3 us -> none  [the longest x1 5.01 us: attention(): jnp.einsum('bkgj,bjkv->bkgv', weights, cache_values, preferred_element_ty...]
    unnamed x21 -> x5, local copies, waits for them, and re-layouts: 21.5 us -> 7.82 us
    all_to_all x1 -> x0, starting transfers between devices: 4.01 us -> none  [moved_by_axis(): filled = lax.all_to_all(filled, axes[k], k, k, tiled=True)]
  transfers between devices with their start and end apart: 3 -> 0, of which waited for: 3 -> 0; matrix products, arithmetic and copies ran while one was open for 16% -> 0% of each run, Pallas kernels for 0% -> 0%
where the time goes in v1:
time: 150 us
  Pallas kernels  139 us (93%)
  local copies, waits for them, and re-layouts  10.4 us (7%)
    pallas_call x1, Pallas kernels, local(): pl.pallas_call(functools.partial(kernel, nz, kv), out_shape=jax.ShapeDtyp...  139 us
    unnamed x5, local copies, waits for them, and re-layouts  7.82 us

profile of v1, /device:TPU:70, one launch (start us, length us, event | category | flops | bytes accessed | tf_op | source)
XLA Modules:
  0.0 149.7 jit_solution(14388327980158914845)
XLA Ops:
  0.0 1.3 reshape.15.ng_ref
  1.3 1.3 reshape.17.mg_ref
  2.6 1.4 copy.18.routes_ref
  3.9 1.3 copy.19.rw_ref
  5.3 1.7 %copy.21.wo_hbm = bf16[1024,64]{1,0:T(8,128)(2,1)} copy(bf16[1024,64]{0,1:T(8,128)(2,1)} %param.22) | data formatting | bytes 262144 | tf_op args[5]
  7.0 1.9 %copy.20.wq_hbm = bf16[2048,32]{1,0:T(8,128)(2,1)} copy(bf16[2048,32]{0,1:T(8,128)(2,1)} %param.19) | data formatting | bytes 262144 | tf_op args[2]
  8.9 139.3 %shard_map.163 = bf16[16,2048]{1,0:T(8,128)(2,1)} custom-call(f32[8]{0:T(128)} %lam_ref.1, s32[16]{0:T(128)} %len_ref.1, bf16[16,2048]{1,0:T(8,128)(2,1)} %tok_ref.1, bf16[1,2048]{1,0:T(2,128)(2,1)} %reshape.15.ng_ref, bf16[1,128]{1,0:T(2,128)(2,1)} %bitcast.5, bf16[1,2048]{1,0:T(2,128)(2,1)} %reshape.17.mg_ref, s32[16,4]{1,0:T(8,128)} %copy.18.routes_ref, ...), custom_call_target="tpu_custom_call" | custom-call | tf_op jit(solution)/shard_map/pallas_call | solution.py:457
  148.2 1.5 copy.23
